TPU v7x, 32 devices: a whole 2x2x4 slice. The times are simulated.
32 devices in a mesh: grp: 2 (over y), sp: 4 (over z), tp: 4 (over x, core).
Axes of the slice: x: 2, y: 2, z: 4, core: 2. Of those that a mesh axis runs over, the one named last changes fastest.
Arguments:
- residual_in: bfloat16 [2048, 2048], P(('grp', 'sp', 'tp')), parts along dimension 0, may hold values from -6 to 6
- query_rows: bfloat16 [2048, 2048], P(('grp', 'sp'), 'tp'), parts along dimension 0, may hold values from -6 to 6
- key_rows: bfloat16 [2048, 512], P(('grp', 'sp'), 'tp'), parts along dimension 0, may hold values from -6 to 6
- value_rows: bfloat16 [2048, 512], P(('grp', 'sp'), 'tp'), parts along dimension 0, may hold values from -6 to 6
- forget_cumsum: float32 [2048, 16], P(('grp', 'sp'), 'tp'), parts along dimension 0, as said below
- head_gain: float32 [2048], P('tp'), may hold values from 0.1 to 1.9
- w_out: bfloat16 [2048, 2048], P('tp'), may hold values from -0.125 to 0.125
- w_up: bfloat16 [2048, 8192], P('sp', 'tp'), may hold values from -0.125 to 0.125
- w_down: bfloat16 [8192, 2048], P('tp', 'sp'), may hold values from -0.0625 to 0.0625
- mixer_gain: float32 [2048], replicated, may hold values from 0.1 to 1.9
- channel_gain: float32 [2048], replicated, may hold values from 0.1 to 1.9
Outputs:
- layer_out: bfloat16 [2048, 2048], P(('grp', 'sp', 'tp')), parts along dimension 0
There are 2 independent parts, one for each index of `grp`. A program takes and returns all parts, laid end to end along the dimension named above; an argument that names none is the same for every part. Nothing has to cross between parts.
Inputs may be any that keep to these rules, and one draw needn't show every extreme that they name: `forget_cumsum`: Non-positive; along the positions, each head's entries never rise.
All inputs are finite; a program needn't handle non-finite values.
Results may differ from a plain program's by a relative error of at most 0.015.
Values may be sent and summed in bfloat16 or wider, within the bound.
A program may use at most 128 MiB of HBM per device.

v0:
```python
import jax
import jax.numpy as jnp
from jax import lax
from jax.sharding import PartitionSpec as P

HD = 128
ALPHA = 8.0**0.25
EPSILON = 1e-05
NEG_FILL = -1e30


def layer_scale(inputs, gain_vec):
    centered = inputs - jnp.mean(inputs, axis=-1, keepdims=True)
    variance = jnp.mean(centered * centered, axis=-1, keepdims=True)
    return centered * lax.rsqrt(variance + EPSILON) * gain_vec


def shards(
    residual_in,
    query_rows,
    key_rows,
    value_rows,
    forget_cumsum,
    head_gain,
    w_out,
    w_up,
    w_down,
    mixer_gain,
    channel_gain,
):
    tok_rows = query_rows.shape[0]
    heads_here = forget_cumsum.shape[1]
    kv_here = key_rows.shape[1] // HD
    group_size = heads_here // kv_here
    score_scale = HD ** (-0.5)
    seq_index = lax.axis_index("sp")
    gate_all = lax.all_gather(forget_cumsum, "sp", axis=0, tiled=True)
    query_grid = query_rows.reshape(tok_rows, kv_here, group_size, HD)
    query_pos = seq_index * tok_rows + jnp.arange(tok_rows, dtype=jnp.int32)
    last_query = seq_index * tok_rows + tok_rows - 1
    gate_query = forget_cumsum.reshape(tok_rows, kv_here, group_size).transpose(1, 2, 0)

    def attend(carry_state, key_block, value_block, first_row):
        row_count = key_block.shape[0]

        def attend_live(live_state):
            peak_score, denom_sum, accum = live_state
            key_grid = key_block.reshape(row_count, kv_here, HD)
            value_grid = value_block.reshape(row_count, kv_here, HD)
            gate_block = lax.dynamic_slice_in_dim(gate_all, first_row, row_count, 0)
            gate_block = gate_block.reshape(row_count, kv_here, group_size).transpose(1, 2, 0)
            scores = (
                jnp.einsum(
                    "tkgd,ukd->kgtu", query_grid, key_grid, preferred_element_type=jnp.float32
                )
                * score_scale
            )
            scores = scores + gate_query[..., None] - gate_block[:, :, None, :]
            key_pos = first_row + jnp.arange(row_count, dtype=jnp.int32)
            allowed = key_pos[None, :] <= query_pos[:, None]
            scores = jnp.where(allowed, scores, NEG_FILL)
            new_peak = jnp.maximum(peak_score, jnp.max(scores, axis=-1))
            weights = jnp.where(allowed, jnp.exp(scores - new_peak[..., None]), 0.0)
            fade_factor = jnp.exp(peak_score - new_peak)
            denom_sum = denom_sum * fade_factor + jnp.sum(weights, axis=-1)
            accum = accum * fade_factor[..., None] + jnp.einsum(
                "kgtu,ukd->kgtd",
                weights.astype(jnp.bfloat16),
                value_grid,
                preferred_element_type=jnp.float32,
            )
            return (new_peak, denom_sum, accum)

        return lax.cond(
            first_row <= last_query, attend_live, lambda kept_state: kept_state, carry_state
        )

    def fold_keys(carry_state, pieces, first_row):
        key_piece, value_piece = pieces
        row_count = key_piece.shape[0]
        block_span = 1024
        if row_count > block_span and row_count % block_span == 0:

            def scan_block(scan_state, block_index):
                offset = block_index * block_span
                next_state = attend(
                    scan_state,
                    lax.dynamic_slice_in_dim(key_piece, offset, block_span, 0),
                    lax.dynamic_slice_in_dim(value_piece, offset, block_span, 0),
                    first_row + offset,
                )
                return (next_state, None)

            carry_state, unused = lax.scan(
                scan_block, carry_state, jnp.arange(row_count // block_span, dtype=jnp.int32)
            )
            return carry_state
        return attend(carry_state, key_piece, value_piece, first_row)

    fold_init = (
        jnp.full((kv_here, group_size, tok_rows), NEG_FILL, jnp.float32),
        jnp.zeros((kv_here, group_size, tok_rows), jnp.float32),
        jnp.zeros((kv_here, group_size, tok_rows, HD), jnp.float32),
    )
    peak_score, denom_sum, accum = fold_keys(
        fold_init,
        (
            lax.all_gather(key_rows, "sp", axis=0, tiled=True),
            lax.all_gather(value_rows, "sp", axis=0, tiled=True),
        ),
        jnp.int32(0),
    )
    attended = accum / denom_sum[..., None]
    normed = attended * lax.rsqrt(jnp.mean(attended * attended, axis=-1, keepdims=True) + EPSILON)
    normed = normed * head_gain.reshape(kv_here, group_size, 1, HD)
    heads_out = normed.transpose(2, 0, 1, 3).reshape(tok_rows, heads_here * HD).astype(jnp.bfloat16)
    branch = lax.psum_scatter(
        jnp.dot(heads_out, w_out, preferred_element_type=jnp.float32).astype(jnp.bfloat16),
        "tp",
        scatter_dimension=0,
        tiled=True,
    ).astype(jnp.float32)
    mid_rows = layer_scale(ALPHA * residual_in.astype(jnp.float32) + branch, mixer_gain).astype(
        jnp.bfloat16
    )
    mid_all = lax.all_gather(mid_rows, "tp", axis=0, tiled=True)
    up_full, down_full = (
        lax.all_gather(w_up, "sp", axis=0, tiled=True),
        lax.all_gather(w_down, "sp", axis=1, tiled=True),
    )
    lifted = jnp.dot(mid_all, up_full, preferred_element_type=jnp.float32)
    active = jnp.square(jax.nn.relu(lifted)).astype(jnp.bfloat16)
    lowered = lax.psum_scatter(
        jnp.dot(active, down_full, preferred_element_type=jnp.float32).astype(jnp.bfloat16),
        "tp",
        scatter_dimension=0,
        tiled=True,
    ).astype(jnp.float32)
    return layer_scale(ALPHA * mid_rows.astype(jnp.float32) + lowered, channel_gain).astype(
        jnp.bfloat16
    )


def solution(mesh):
    placed = (
        P(("grp", "sp", "tp"), None),
        P(("grp", "sp"), "tp"),
        P(("grp", "sp"), "tp"),
        P(("grp", "sp"), "tp"),
        P(("grp", "sp"), "tp"),
        P("tp"),
        P("tp", None),
        P("sp", "tp"),
        P("tp", "sp"),
        P(),
        P(),
    )
    return jax.shard_map(
        shards, mesh=mesh, in_specs=placed, out_specs=P(("grp", "sp", "tp"), None), check_vma=False
    )
```

profile of v0, /device:TPU:0, one launch (start us, length us, event | category | flops | bytes accessed | tf_op | source)
XLA Modules:
  0.0 451.6 jit_solution(16163317256759813407)
XLA Ops:
  6.5 0.0 copy-start
  6.5 0.0 reduce-scatter.3.cloned.1.call-start
  6.5 16.0 %all_gather.18 = bf16[1024,128]{1,0:T(8,128)(2,1)S(1)} all-gather(bf16[256,128]{1,0:T(8,128)(2,1)} %param.15), channel_id=1, replica_groups=mesh['grp'=2,'sp'=4,'tp'=4] {'sp'}, dimensions={0}, use_global_device_ids=true | all-gather | bytes 327680 | tf_op jit(solution)/shard_map/all_gather | solution.py:108
  22.5 14.8 %all_gather.20 = bf16[1024,128]{1,0:T(8,128)(2,1)S(1)} all-gather(bf16[256,128]{1,0:T(8,128)(2,1)} %param.16), channel_id=1, replica_groups=mesh['grp'=2,'sp'=4,'tp'=4] {'sp'}, dimensions={0}, use_global_device_ids=true | all-gather | bytes 327680 | tf_op jit(solution)/shard_map/all_gather | solution.py:109
  37.4 13.3 %all_gather.19 = f32[1024,4]{0,1:T(4,128)S(1)} all-gather(f32[256,4]{0,1:T(4,128)} %param.17), channel_id=1, replica_groups=mesh['grp'=2,'sp'=4,'tp'=4] {'sp'}, dimensions={0}, use_global_device_ids=true | all-gather | bytes 20480 | tf_op jit(solution)/shard_map/all_gather | solution.py:37
  50.7 0.0 copy-start.6
  50.7 6.1 %conditional.1 = (f32[1,4,256]{2,1,0:T(4,128)S(1)}, f32[1,4,256,128]{2,3,1,0:T(8,128)S(1)}) conditional(s32[]{:T(128)} %convert_element_type.43, () %tuple.13, (s32[]{:T(128)}, s32[256]{0:T(256)S(1)}, bf16[256,512]{1,0:T(8,128)(2,1)}, bf16[1024,128]{1,0:T(8,128)(2,1)S(1)}, f32[1,4,256]{2,1,0:T(4,128)}, /*index=5*/f32[1024,4]{0,1:T(4,128)S(1)}, ...), branch_computations={%region_0.0_spmd, %region_1.4_spmd} | conditional | flops 557190400 | bytes 16116784 | solution.py:74
  50.7 0.0 copy-start.3
  50.7 0.2 iota_compare_fusion
  50.9 2.1 fusion.4
  53.0 0.0 copy-done.3
  53.0 1.5 fusion.3
  54.5 2.1 fusion.12
  56.6 0.2 copy.20
  56.8 0.0 copy-start.2
  56.8 0.0 copy-start.4
  56.8 0.1 multiply_reduce_fusion.2
  56.9 0.0 copy-done.6
  56.9 0.1 multiply_convert_fusion.2
  57.1 0.0 copy-done
  57.1 1.7 convolution_convert_fusion
  58.8 0.0 reduce-scatter.3.cloned.1.call-update
  58.8 0.0 all-gather.4.cloned.1.call-start
  58.9 25.8 %reduce-scatter.3.cloned.1.call-done = bf16[64,2048]{1,0:T(8,128)(2,1)} async-done(((bf16[256,2048]{1,0:T(8,128)(2,1)}), bf16[64,2048]{1,0:T(8,128)(2,1)}) %reduce-scatter.3.cloned.1.call-update) | async-done | bytes 262160 | tf_op jit(solution)/shard_map/reduce_scatter | solution.py:117
  84.7 0.0 copy-done.2
  84.7 1.1 fusion.25
  85.9 1.2 multiply_reduce_fusion.1
  87.0 0.0 copy-done.4
  87.1 1.8 multiply_convert_fusion.1
  88.9 0.0 all-gather.4.cloned.1.call-update
  88.9 0.0 all-gather.6.cloned.1.call-start
  88.9 0.7 all-gather.6.cloned.1.call-update
  89.6 0.0 all-gather.8.cloned.1.call-start
  89.7 0.5 all-gather.8.cloned.1.call-update
  90.2 0.0 copy-start.1
  90.2 0.0 copy-start.5
  90.2 0.0 reduce-scatter.5.cloned.1.call-start
  90.3 15.5 %all-gather.4.cloned.1.call-done = bf16[256,2048]{1,0:T(8,128)(2,1)} async-done(((bf16[64,2048]{1,0:T(8,128)(2,1)}), bf16[256,2048]{1,0:T(8,128)(2,1)}) %all-gather.4.cloned.1.call-update) | async-done | bytes 1048592 | tf_op jit(solution)/shard_map/all_gather | solution.py:126
  105.7 151.2 %all-gather.6.cloned.1.call-done = bf16[2048,2048]{1,0:T(8,128)(2,1)} async-done(((bf16[512,2048]{1,0:T(8,128)(2,1)}), bf16[2048,2048]{1,0:T(8,128)(2,1)}) %all-gather.6.cloned.1.call-update) | async-done | bytes 8388624 | tf_op jit(solution)/shard_map/all_gather | solution.py:128
  257.0 149.3 %all-gather.8.cloned.1.call-done = bf16[2048,2048]{1,0:T(8,128)(2,1)} async-done(((bf16[2048,512]{1,0:T(8,128)(2,1)}), bf16[2048,2048]{1,0:T(8,128)(2,1)}) %all-gather.8.cloned.1.call-update) | async-done | bytes 8388624 | tf_op jit(solution)/shard_map/all_gather | solution.py:129
  406.2 11.6 %convolution_convert_fusion.1 = bf16[256,2048]{1,0:T(8,128)(2,1)} fusion(bf16[2048,2048]{1,0:T(8,128)(2,1)} %all-gather.8.cloned.1.call-done, bf16[256,2048]{1,0:T(8,128)(2,1)} %all-gather.4.cloned.1.call-done, bf16[2048,2048]{1,0:T(8,128)(2,1)} %all-gather.6.cloned.1.call-done), kind=kOutput, calls=%fused_computation.29 | convolution fusion | flops 4297064448 | bytes 18874368 | tf_op jit(solution)/shard_map/dot_general | solution.py:134
  417.8 0.0 reduce-scatter.5.cloned.1.call-update
  417.8 23.1 %reduce-scatter.5.cloned.1.call-done = bf16[64,2048]{1,0:T(8,128)(2,1)} async-done(((bf16[256,2048]{1,0:T(8,128)(2,1)}), bf16[64,2048]{1,0:T(8,128)(2,1)}) %reduce-scatter.5.cloned.1.call-update) | async-done | bytes 262160 | tf_op jit(solution)/shard_map/reduce_scatter | solution.py:133
  440.9 0.0 copy-done.1
  440.9 1.1 fusion.26
  442.0 1.2 multiply_reduce_fusion
  443.2 0.0 copy-done.5
  443.2 1.8 multiply_convert_fusion
  (9 shorter events, 0.1 us)
Async XLA Ops:
  6.5 50.5 %copy-start = (bf16[512,2048]{1,0:T(8,128)(2,1)S(1)}, bf16[512,2048]{1,0:T(8,128)(2,1)}, u32[]{:S(2)}) copy-start(bf16[512,2048]{1,0:T(8,128)(2,1)} %param.19) | copy-start | bytes 6291460
  6.5 78.2 %reduce-scatter.3.cloned.1.call-start = ((), (), s32[]{:S(2)}) async-start(), calls=%async_computation.2 | async-start | bytes 1310720 | tf_op jit(solution)/shard_map/reduce_scatter | solution.py:117
  50.7 6.2 %copy-start.6 = (f32[512]{0:T(512)S(1)}, f32[512]{0:T(512)}, u32[]{:S(2)}) copy-start(f32[512]{0:T(512)} %param.18) | copy-start | bytes 6148
  50.7 2.3 copy-start.3
  56.8 27.9 %copy-start.2 = (bf16[64,2048]{1,0:T(8,128)(2,1)S(1)}, bf16[64,2048]{1,0:T(8,128)(2,1)}, u32[]{:S(2)}) copy-start(bf16[64,2048]{1,0:T(8,128)(2,1)} %param.13) | copy-start | bytes 786436
  56.8 30.2 %copy-start.4 = (f32[2048]{0:T(1024)S(1)}, f32[2048]{0:T(1024)}, u32[]{:S(2)}) copy-start(f32[2048]{0:T(1024)} %param.22) | copy-start | bytes 24580
  58.8 46.9 %all-gather.4.cloned.1.call-start = ((), (), s32[]{:S(2)}) async-start(), calls=%async_computation.3 | async-start | bytes 1310720 | tf_op jit(solution)/shard_map/all_gather | solution.py:126
  88.9 168.1 %all-gather.6.cloned.1.call-start = ((), (), s32[]{:S(2)}) async-start(), calls=%async_computation.4 | async-start | bytes 10485760 | tf_op jit(solution)/shard_map/all_gather | solution.py:128
  89.6 316.6 %all-gather.8.cloned.1.call-start = ((), (), s32[]{:S(2)}) async-start(), calls=%async_computation.5 | async-start | bytes 10485760 | tf_op jit(solution)/shard_map/all_gather | solution.py:129
  90.2 350.7 %copy-start.1 = (bf16[64,2048]{1,0:T(8,128)(2,1)S(1)}, bf16[64,2048]{1,0:T(8,128)(2,1)}, u32[]{:S(2)}) copy-start(bf16[64,2048]{1,0:T(8,128)(2,1)} %multiply_convert_fusion.1) | copy-start | bytes 786436
  90.2 353.0 %copy-start.5 = (f32[2048]{0:T(1024)S(1)}, f32[2048]{0:T(1024)}, u32[]{:S(2)}) copy-start(f32[2048]{0:T(1024)} %param.23) | copy-start | bytes 24580
  90.2 350.7 %reduce-scatter.5.cloned.1.call-start = ((), (), s32[]{:S(2)}) async-start(), calls=%async_computation.6 | async-start | bytes 1310720 | tf_op jit(solution)/shard_map/reduce_scatter | solution.py:133
Sparse Core Ops, SparseCore 0:
  59.0 25.7 reduce-scatter.2
  89.0 16.6 all-gather.3
  107.3 149.6 all-gather.5
  258.4 147.7 all-gather.7
  417.9 22.9 reduce-scatter.4
where the time goes:
time: 452 us
  waiting for transfers between devices  366 us (81%)
  blocking collectives  44.2 us (10%)
  matrix products  17.5 us (4%)
  between operations  13.3 us (3%)
  other arithmetic  10.1 us (2%)
    all_gather x1, waiting for transfers between devices, shards(): lax.all_gather(w_up, 'sp', axis=0, tiled=True)  151 us
    all_gather x1, waiting for transfers between devices, shards(): lax.all_gather(w_down, 'sp', axis=1, tiled=True)  149 us
    reduce_scatter x1, waiting for transfers between devices, shards(): lax.psum_scatter(jnp.dot(heads_out, w_out, preferred_element_type=jnp.flo...  25.8 us
    reduce_scatter x1, waiting for transfers between devices, shards(): lax.psum_scatter(jnp.dot(active, down_full, preferred_element_type=jnp.fl...  23.1 us
    all_gather x1, blocking collectives, shards(): lax.all_gather(key_rows, 'sp', axis=0, tiled=True)  16 us
    all_gather x1, waiting for transfers between devices, shards(): mid_all = lax.all_gather(mid_rows, 'tp', axis=0, tiled=True)  15.5 us
    all_gather x1, blocking collectives, shards(): lax.all_gather(value_rows, 'sp', axis=0, tiled=True)  14.8 us
    all_gather x1, blocking collectives, shards(): gate_all = lax.all_gather(forget_cumsum, 'sp', axis=0, tiled=True)  13.3 us
  transfers between devices with their start and end apart: 5, of which 5 were waited for; matrix products, arithmetic and copies ran while one was open for 0% of the time, Pallas kernels for 0%

commit v1 on v0

--- a/solution.py
+++ b/solution.py
@@ -126,7 +126,7 @@
     mid_all = lax.all_gather(mid_rows, "tp", axis=0, tiled=True)
     up_full, down_full = (
         lax.all_gather(w_up, "sp", axis=0, tiled=True),
-        lax.all_gather(w_down, "sp", axis=1, tiled=True),
+        jnp.concatenate(lax.all_gather(w_down, "sp"), axis=1),
     )
     lifted = jnp.dot(mid_all, up_full, preferred_element_type=jnp.float32)
     active = jnp.square(jax.nn.relu(lifted)).astype(jnp.bfloat16)

time: 452 us -> 427 us (0.945)
  waiting for transfers between devices: 366 us -> 326 us
  local copies, waits for them, and re-layouts: 0.24 us -> 11.7 us
    all_gather x1, waiting for transfers between devices: 149 us -> 122 us  [shards(): lax.all_gather(w_down, 'sp')]
    reshape x0 -> x1, local copies, waits for them, and re-layouts: none -> 11.5 us  [shards(): jnp.concatenate(lax.all_gather(w_down, 'sp'), axis=1)]
    all_gather x1, waiting for transfers between devices: 15.5 us -> 4.73 us  [shards(): mid_all = lax.all_gather(mid_rows, 'tp', axis=0, tiled=True)]
  transfers between devices with their start and end apart: 5 -> 5, of which waited for: 5 -> 5; matrix products, arithmetic and copies ran while one was open for 0% -> 4% of each run, Pallas kernels for 0% -> 0%
where the time goes in v1:
time: 427 us
  waiting for transfers between devices  326 us (76%)
  blocking collectives  45.7 us (11%)
  matrix products  17.6 us (4%)
  between operations  15.1 us (4%)
  local copies, waits for them, and re-layouts  11.7 us (3%)
  other arithmetic  10.1 us (2%)
    all_gather x1, waiting for transfers between devices, shards(): lax.all_gather(w_up, 'sp', axis=0, tiled=True)  151 us
    all_gather x1, waiting for transfers between devices, shards(): lax.all_gather(w_down, 'sp')  122 us
    reduce_scatter x1, waiting for transfers between devices, shards(): lax.psum_scatter(jnp.dot(heads_out, w_out, preferred_element_type=jnp.flo...  24.4 us
    reduce_scatter x1, waiting for transfers between devices, shards(): lax.psum_scatter(jnp.dot(active, down_full, preferred_element_type=jnp.fl...  23.1 us
    all_gather x1, blocking collectives, shards(): lax.all_gather(value_rows, 'sp', axis=0, tiled=True)  16.4 us
    all_gather x1, blocking collectives, shards(): lax.all_gather(key_rows, 'sp', axis=0, tiled=True)  16 us
    all_gather x1, blocking collectives, shards(): gate_all = lax.all_gather(forget_cumsum, 'sp', axis=0, tiled=True)  13.3 us
    dot_general x1, matrix products, shards(): jnp.dot(active, down_full, preferred_element_type=jnp.float32)  11.6 us
  transfers between devices with their start and end apart: 5, of which 5 were waited for; matrix products, arithmetic and copies ran while one was open for 4% of the time, Pallas kernels for 0%

profile of v1, /device:TPU:0, one launch (start us, length us, event | category | flops | bytes accessed | tf_op | source)
XLA Modules:
  0.0 426.6 jit_solution(2649168089818737585)
XLA Ops:
  7.4 0.0 copy-start
  7.4 0.0 reduce-scatter.3.cloned.1.call-start
  7.4 16.0 %all_gather.21 = bf16[1024,128]{1,0:T(8,128)(2,1)S(1)} all-gather(bf16[256,128]{1,0:T(8,128)(2,1)} %param.15), channel_id=1, replica_groups=mesh['grp'=2,'sp'=4,'tp'=4] {'sp'}, dimensions={0}, use_global_device_ids=true | all-gather | bytes 327680 | tf_op jit(solution)/shard_map/all_gather | solution.py:108
  23.4 16.4 %all_gather.23 = bf16[1024,128]{1,0:T(8,128)(2,1)} all-gather(bf16[256,128]{1,0:T(8,128)(2,1)} %param.16), channel_id=1, replica_groups=mesh['grp'=2,'sp'=4,'tp'=4] {'sp'}, dimensions={0}, use_global_device_ids=true | all-gather | bytes 327680 | tf_op jit(solution)/shard_map/all_gather | solution.py:109
  39.7 13.3 %all_gather.22 = f32[1024,4]{0,1:T(4,128)S(1)} all-gather(f32[256,4]{0,1:T(4,128)} %param.17), channel_id=1, replica_groups=mesh['grp'=2,'sp'=4,'tp'=4] {'sp'}, dimensions={0}, use_global_device_ids=true | all-gather | bytes 20480 | tf_op jit(solution)/shard_map/all_gather | solution.py:37
  53.1 0.0 copy-start.7
  53.1 6.1 %conditional.1 = (f32[1,4,256]{2,1,0:T(4,128)S(1)}, f32[1,4,256,128]{2,3,1,0:T(8,128)S(1)}) conditional(s32[]{:T(128)} %convert_element_type.43, () %tuple.13, (s32[]{:T(128)}, s32[256]{0:T(256)S(1)}, bf16[256,512]{1,0:T(8,128)(2,1)}, bf16[1024,128]{1,0:T(8,128)(2,1)S(1)}, f32[1,4,256]{2,1,0:T(4,128)}, /*index=5*/f32[1024,4]{0,1:T(4,128)S(1)}, ...), branch_computations={%region_0.0_spmd, %region_1.4_spmd} | conditional | flops 557190400 | bytes 17165388 | solution.py:74
  53.1 0.2 iota_compare_fusion
  53.3 0.0 copy-start.3
  53.3 2.1 fusion.4
  55.4 0.0 copy-done.4
  55.4 1.5 fusion.3
  56.9 0.0 copy-done.3
  57.0 2.0 fusion.12
  59.0 0.2 copy.24
  59.2 0.0 copy-start.2
  59.2 0.1 multiply_reduce_fusion.2
  59.3 0.0 copy-done.7
  59.3 0.0 copy-start.5
  59.3 0.1 multiply_convert_fusion.2
  59.5 0.0 copy-done
  59.5 1.8 convolution_convert_fusion
  61.3 0.0 reduce-scatter.3.cloned.1.call-update
  61.3 0.0 all-gather.9.cloned.1.call-start
  61.4 0.5 all-gather.9.cloned.1.call-update
  61.9 0.0 all-gather.5.cloned.1.call-start
  61.9 24.4 %reduce-scatter.3.cloned.1.call-done = bf16[64,2048]{1,0:T(8,128)(2,1)} async-done(((bf16[256,2048]{1,0:T(8,128)(2,1)}), bf16[64,2048]{1,0:T(8,128)(2,1)}) %reduce-scatter.3.cloned.1.call-update) | async-done | bytes 262160 | tf_op jit(solution)/shard_map/reduce_scatter | solution.py:117
  86.3 0.0 copy-done.2
  86.3 1.1 fusion.25
  87.5 1.2 multiply_reduce_fusion.1
  88.7 0.0 copy-done.5
  88.7 1.8 multiply_convert_fusion.1
  90.5 0.0 all-gather.5.cloned.1.call-update
  90.5 0.0 all-gather.7.cloned.1.call-start
  90.5 0.5 all-gather.7.cloned.1.call-update
  91.1 0.0 reduce-scatter.5.cloned.1.call-start
  91.1 121.8 %all-gather.9.cloned.1.call-done = bf16[8192,512]{1,0:T(8,128)(2,1)} async-done(((bf16[2048,512]{1,0:T(8,128)(2,1)}), bf16[8192,512]{1,0:T(8,128)(2,1)}) %all-gather.9.cloned.1.call-update) | async-done | bytes 8388624 | tf_op jit(solution)/shard_map/all_gather | solution.py:129
  212.9 11.5 %copy.21 = bf16[2048,4,512]{0,2,1:T(8,128)(2,1)} copy(bf16[2048,4,512]{2,0,1:T(8,128)(2,1)} %bitcast.72) | data formatting | bytes 16777216 | tf_op jit(solution)/shard_map/reshape | solution.py:129
  224.4 4.7 %all-gather.5.cloned.1.call-done = bf16[256,2048]{1,0:T(8,128)(2,1)} async-done(((bf16[64,2048]{1,0:T(8,128)(2,1)}), bf16[256,2048]{1,0:T(8,128)(2,1)}) %all-gather.5.cloned.1.call-update) | async-done | bytes 1048592 | tf_op jit(solution)/shard_map/all_gather | solution.py:126
  229.1 150.9 %all-gather.7.cloned.1.call-done = bf16[2048,2048]{1,0:T(8,128)(2,1)} async-done(((bf16[512,2048]{1,0:T(8,128)(2,1)}), bf16[2048,2048]{1,0:T(8,128)(2,1)}) %all-gather.7.cloned.1.call-update) | async-done | bytes 8388624 | tf_op jit(solution)/shard_map/all_gather | solution.py:128
  380.1 11.6 %convolution_convert_fusion.1 = bf16[256,2048]{1,0:T(8,128)(2,1)} fusion(bf16[2048,2048]{0,1:T(8,128)(2,1)} %bitcast.73, bf16[256,2048]{1,0:T(8,128)(2,1)} %all-gather.5.cloned.1.call-done, bf16[2048,2048]{1,0:T(8,128)(2,1)} %all-gather.7.cloned.1.call-done), kind=kOutput, calls=%fused_computation.29 | convolution fusion | flops 4297064448 | bytes 18874368 | tf_op jit(solution)/shard_map/dot_general | solution.py:134
  391.7 0.0 reduce-scatter.5.cloned.1.call-update
  391.7 23.1 %reduce-scatter.5.cloned.1.call-done = bf16[64,2048]{1,0:T(8,128)(2,1)} async-done(((bf16[256,2048]{1,0:T(8,128)(2,1)}), bf16[64,2048]{1,0:T(8,128)(2,1)}) %reduce-scatter.5.cloned.1.call-update) | async-done | bytes 262160 | tf_op jit(solution)/shard_map/reduce_scatter | solution.py:133
  414.8 0.0 copy-done.1
  414.8 1.1 fusion.26
  416.0 1.2 multiply_reduce_fusion
  417.2 0.0 copy-done.6
  417.2 1.8 multiply_convert_fusion
  (12 shorter events, 0.1 us)
Async XLA Ops:
  7.4 52.1 %copy-start = (bf16[512,2048]{1,0:T(8,128)(2,1)S(1)}, bf16[512,2048]{1,0:T(8,128)(2,1)}, u32[]{:S(2)}) copy-start(bf16[512,2048]{1,0:T(8,128)(2,1)} %param.19) | copy-start | bytes 6291460
  7.4 78.9 %reduce-scatter.3.cloned.1.call-start = ((), (), s32[]{:S(2)}) async-start(), calls=%async_computation.2 | async-start | bytes 1310720 | tf_op jit(solution)/shard_map/reduce_scatter | solution.py:117
  53.1 6.2 %copy-start.7 = (f32[512]{0:T(512)S(1)}, f32[512]{0:T(512)}, u32[]{:S(2)}) copy-start(f32[512]{0:T(512)} %param.18) | copy-start | bytes 6148
  53.1 2.4 copy-start.4
  53.3 3.7 copy-start.3
  59.2 27.1 %copy-start.2 = (bf16[64,2048]{1,0:T(8,128)(2,1)S(1)}, bf16[64,2048]{1,0:T(8,128)(2,1)}, u32[]{:S(2)}) copy-start(bf16[64,2048]{1,0:T(8,128)(2,1)} %param.13) | copy-start | bytes 786436
  59.3 29.3 %copy-start.5 = (f32[2048]{0:T(1024)S(1)}, f32[2048]{0:T(1024)}, u32[]{:S(2)}) copy-start(f32[2048]{0:T(1024)} %param.22) | copy-start | bytes 24580
  61.3 151.6 %all-gather.9.cloned.1.call-start = ((), (), s32[]{:S(2)}) async-start(), calls=%async_computation.6 | async-start | bytes 10485760 | tf_op jit(solution)/shard_map/all_gather | solution.py:129
  61.9 167.2 %all-gather.5.cloned.1.call-start = ((), (), s32[]{:S(2)}) async-start(), calls=%async_computation.3 | async-start | bytes 1310720 | tf_op jit(solution)/shard_map/all_gather | solution.py:126
  90.5 289.6 %all-gather.7.cloned.1.call-start = ((), (), s32[]{:S(2)}) async-start(), calls=%async_computation.4 | async-start | bytes 10485760 | tf_op jit(solution)/shard_map/all_gather | solution.py:128
  91.1 323.8 %reduce-scatter.5.cloned.1.call-start = ((), (), s32[]{:S(2)}) async-start(), calls=%async_computation.5 | async-start | bytes 1310720 | tf_op jit(solution)/shard_map/reduce_scatter | solution.py:133
  380.1 34.7 %copy-start.1 = (bf16[64,2048]{1,0:T(8,128)(2,1)S(1)}, bf16[64,2048]{1,0:T(8,128)(2,1)}, u32[]{:S(2)}) copy-start(bf16[64,2048]{1,0:T(8,128)(2,1)} %multiply_convert_fusion.1) | copy-start | bytes 786436
  380.1 37.1 %copy-start.6 = (f32[2048]{0:T(1024)S(1)}, f32[2048]{0:T(1024)}, u32[]{:S(2)}) copy-start(f32[2048]{0:T(1024)} %param.23) | copy-start | bytes 24580
Sparse Core Ops, SparseCore 0:
  61.4 24.8 reduce-scatter.2
  391.9 22.9 reduce-scatter.4
Sparse Core Ops, SparseCore 1:
  63.4 149.5 all-gather.8
  214.4 14.7 all-gather.4
  230.6 149.4 all-gather.6
